TPU v7x, 256 devices: a whole 4x4x8 slice. The times are simulated.
256 devices in a mesh: ep: 16 (over y, x), tp: 16 (over z, core).
Axes of the slice: x: 4, y: 4, z: 8, core: 2. Of those that a mesh axis runs over, the one named last changes fastest.
Arguments:
- tokens: bfloat16 [8192, 1024], P(('ep', 'tp')), may hold values from -6 to 6
- norm_gain: float32 [1024], replicated, may hold values from 0.5 to 1.5
- routing: int32 [8192, 2], P('ep'), may hold values from 0 to 31, as said below
- gate_share: float32 [8192, 2], P('ep'), may hold values from 0.5 to 1.5
- w_gate: bfloat16 [32, 1024, 256], P('ep', None, 'tp'), may hold values from -0.1875 to 0.1875
- w_up: bfloat16 [32, 1024, 256], P('ep', None, 'tp'), may hold values from -0.1875 to 0.1875
- w_down: bfloat16 [32, 256, 1024], P('ep', 'tp'), may hold values from -0.375 to 0.375
Outputs:
- mixed_out: bfloat16 [8192, 1024], P('ep', 'tp')
Inputs may be any that keep to these rules, and one draw needn't show every extreme that they name: `routing`: each row names two different experts whose ids lie in the same block of 8 consecutive ids. In each aligned block of 512 rows (the tokens of one index of ep) no expert is named by more than 64 rows, and some expert is named by exactly 64.
All inputs are finite; a program needn't handle non-finite values.
Results may differ from a plain program's by a relative error of at most 0.0015.
Values may be sent and summed in bfloat16 or wider, within the bound.
No kernel may reach another device: no remote copies, remote signals or barrier semaphores. Data moves between devices by JAX's collectives and lax.ppermute only.
A program may use at most 64 MiB of HBM per device.

v0:
```python
import jax
import jax.numpy as jnp
from jax import lax
from jax.sharding import PartitionSpec as P

epsilon = 1e-06


def in_order(parts, dim):
    shape = list(parts.shape[1:])
    shape[dim] *= parts.shape[0]
    return jnp.moveaxis(parts, 0, dim).reshape(shape)


def gather_together(arrays, axis, dims):
    flat = jnp.concatenate([a.reshape(-1) for a in arrays])
    lines, at, outs = lax.all_gather(flat, axis), 0, []
    for a, dim in zip(arrays, dims):
        parts = lines[:, at : at + a.size].reshape(-1, *a.shape)
        outs.append(in_order(parts, dim))
        at += a.size
    return tuple(outs)


def norm_rows(tokens, norm_gain):
    as_float = tokens.astype(jnp.float32)
    scaled = as_float * lax.rsqrt(jnp.mean(as_float * as_float, axis=-1, keepdims=True) + epsilon)
    return (scaled * norm_gain.astype(jnp.float32)).astype(jnp.bfloat16)


def fill_buffer(group, flat_target, slots, model_width):
    buffer = jnp.zeros((slots, model_width), jnp.bfloat16)
    return buffer.at[flat_target].set(jnp.repeat(group, 2, axis=0))


def body(tokens, norm_gain, routing, gate_share, w_gate, w_up, w_down):
    ep_size = lax.axis_size("ep")
    tp_size = lax.axis_size("tp")
    local_experts = w_gate.shape[0]
    experts = local_experts * ep_size
    group_rows = routing.shape[0]
    capacity = group_rows * 4 // experts
    model_width = tokens.shape[1]
    columns = model_width // tp_size
    normed = norm_rows(tokens, norm_gain)
    onehot = (routing[:, :, None] == jnp.arange(experts, dtype=jnp.int32)[None, None, :]).astype(
        jnp.int32
    )
    flat_hot = onehot.reshape(group_rows * 2, experts)
    ranking = jnp.cumsum(flat_hot, axis=0) - 1
    slot_pos = jnp.sum(ranking * flat_hot, axis=1).reshape(group_rows, 2)
    target = (routing * capacity + slot_pos).astype(jnp.int32)
    flat_target = target.reshape(-1)
    slice_len = capacity // tp_size
    tp_index = lax.axis_index("tp")
    group = lax.all_gather(normed, "tp", axis=0, tiled=True)
    buffer = fill_buffer(group, flat_target, experts * capacity, model_width)
    shaped = buffer.reshape(ep_size, local_experts, capacity, model_width)
    mine = lax.dynamic_slice_in_dim(shaped, tp_index * slice_len, slice_len, 2)
    mine = mine.reshape(ep_size, local_experts * slice_len, model_width)
    landed = lax.all_to_all(mine, "ep", split_axis=0, concat_axis=0, tiled=True)
    landed = landed.reshape(ep_size, local_experts, slice_len, model_width).transpose(1, 0, 2, 3)
    landed = landed.reshape(local_experts, ep_size * slice_len, model_width)
    full_gate, full_up, full_down = gather_together((w_gate, w_up, w_down), "tp", (2, 2, 1))
    gate_sum = jnp.einsum("erd,edh->erh", landed, full_gate, preferred_element_type=jnp.float32)
    up_sum = jnp.einsum("erd,edh->erh", landed, full_up, preferred_element_type=jnp.float32)
    hidden = (jax.nn.silu(gate_sum) * up_sum).astype(jnp.bfloat16)
    produced = jnp.einsum(
        "erh,ehd->erd", hidden, full_down, preferred_element_type=jnp.float32
    ).astype(jnp.bfloat16)
    produced = produced.reshape(local_experts, ep_size, slice_len, model_width)
    blocks = lax.all_to_all(produced, "tp", split_axis=3, concat_axis=2, tiled=True)
    leaving = blocks.transpose(1, 0, 2, 3).reshape(ep_size, local_experts * capacity, columns)
    returned = lax.all_to_all(leaving, "ep", split_axis=0, concat_axis=0, tiled=True).reshape(
        experts * capacity, columns
    )
    picked_out = returned[target]
    mixed_out = jnp.sum(gate_share[:, :, None] * picked_out.astype(jnp.float32), axis=1)
    return mixed_out.astype(jnp.bfloat16)


def solution(mesh):
    return jax.shard_map(
        body,
        mesh=mesh,
        in_specs=(
            P(("ep", "tp"), None),
            P(),
            P("ep", None),
            P("ep", None),
            P("ep", None, "tp"),
            P("ep", None, "tp"),
            P("ep", "tp", None),
        ),
        out_specs=P("ep", "tp"),
        check_vma=False,
    )
```

profile of v0, /device:TPU:1, one launch (start us, length us, event | category | flops | bytes accessed | tf_op | source)
XLA Modules:
  0.0 184.5 jit_solution(3607458096180063243)
XLA Ops:
  6.5 1.0 fusion.4
  7.5 1.6 fusion.6
  9.2 1.1 copy.96
  10.6 1.1 copy.97
  12.1 0.9 copy.115
  12.9 0.7 pad_maximum_fusion
  14.2 9.0 %reduce-window.6 = s32[32,8,128]{2,1,0:T(8,128)S(1)} reduce-window(s32[32,8,128]{2,1,0:T(8,128)S(1)} %fusion.14, s32[]{:T(128)} %constant.13.clone.1), window={size=1x1x128 pad=0_0x0_0x127_0}, to_apply=%region_0.0 | reduce-window | flops 4161536 | bytes 262148 | tf_op jit(solution)/shard_map/reduce-window
  24.4 27.5 %all-gather.4.cloned.1.call-done = bf16[512,1024]{1,0:T(8,128)(2,1)} async-done(((bf16[32,1024]{1,0:T(8,128)(2,1)}), bf16[512,1024]{1,0:T(8,128)(2,1)}) %all-gather.4.cloned.1.call-update) | async-done | bytes 1048592 | tf_op jit(solution)/shard_map/all_gather | solution.py:56
  51.9 2.3 %broadcast_in_dim.7 = bf16[512,2,1024]{2,1,0:T(2,128)(2,1)S(1)} broadcast(bf16[512,1024]{1,0:T(8,128)(2,1)} %all-gather.4.cloned.1.call-done), dimensions={0,2} | broadcast | bytes 3145728 | tf_op jit(solution)/shard_map/broadcast_in_dim | solution.py:33
  54.2 2.3 %reshape.147 = bf16[1024,1024]{1,0:T(8,128)(2,1)} reshape(bf16[512,2,1024]{2,1,0:T(2,128)(2,1)S(1)} %broadcast_in_dim.7) | data formatting | bytes 4194304 | tf_op jit(solution)/shard_map/reshape | solution.py:33
  56.5 8.6 %scatter_custom_fusion = bf16[2048,1024]{1,0:T(8,128)(2,1)} fusion(s32[1024]{0:T(1024)S(1)} %bitcast.70, bf16[1024,1024]{1,0:T(8,128)(2,1)} %reshape.147, bf16[]{:T(256)} %constant.11.clone.1), kind=kCustom, calls=%fused_computation.2 | custom fusion | bytes 4194816 | tf_op jit(solution)/shard_map/scatter | solution.py:33
  65.1 1.2 constant_dynamic-slice_fusion
  66.6 14.5 %all_to_all.28 = bf16[16,8,1024]{2,1,0:T(8,128)(2,1)S(1)} all-to-all(bf16[16,8,1024]{2,1,0:T(8,128)(2,1)S(1)} %copy.93), channel_id=1, replica_groups=mesh['ep'=16,'tp'=16] {'ep'}, dimensions={0} | all-to-all | bytes 524288 | tf_op jit(solution)/shard_map/all_to_all | solution.py:61
  81.6 11.4 %all-gather.6.cloned.1.call-done = bf16[1572864]{0:T(1024)(128)(2,1)} async-done(((bf16[98304]{0:T(1024)(128)(2,1)}), bf16[1572864]{0:T(1024)(128)(2,1)}) %all-gather.6.cloned.1.call-update) | async-done | bytes 3145744 | tf_op jit(solution)/shard_map/all_gather | solution.py:17
  93.0 2.8 %reshape.151 = bf16[16,98304]{1,0:T(8,128)(2,1)S(1)} reshape(bf16[1572864]{0:T(1024)(128)(2,1)} %all-gather.6.cloned.1.call-done) | data formatting | bytes 6291456 | tf_op jit(solution)/shard_map/all_gather | solution.py:17
  95.7 1.8 fusion.17
  97.5 9.6 %reshape.126 = bf16[16,2,1024,16]{3,2,1,0:T(8,128)(2,1)} reshape(bf16[16,32768]{1,0:T(8,128)(2,1)} %get-tuple-element.7) | data formatting | bytes 2097152 | tf_op jit(solution)/shard_map/reshape | solution.py:19
  107.2 6.8 %copy.98 = bf16[2,1024,16,16]{1,3,2,0:T(8,128)(2,1)S(1)} copy(bf16[2,1024,16,16]{3,1,0,2:T(8,128)(2,1)} %bitcast.51) | data formatting | bytes 2097152 | tf_op jit(solution)/shard_map/transpose | solution.py:12
  114.0 8.9 %reshape.128 = bf16[16,2,1024,16]{3,2,1,0:T(8,128)(2,1)} reshape(bf16[16,32768]{1,0:T(8,128)(2,1)S(1)} %copy-done) | data formatting | bytes 2097152 | tf_op jit(solution)/shard_map/reshape | solution.py:19
  122.9 6.8 %copy.100 = bf16[2,1024,16,16]{1,3,2,0:T(8,128)(2,1)S(1)} copy(bf16[2,1024,16,16]{3,1,0,2:T(8,128)(2,1)} %bitcast.52) | data formatting | bytes 2097152 | tf_op jit(solution)/shard_map/transpose | solution.py:12
  130.8 0.7 convolution_convert_fusion
  131.7 1.4 copy.103
  133.1 2.1 %reshape.157 = bf16[16,2,4096]{2,1,0:T(2,128)(2,1)S(1)} reshape(bf16[1024,2,4,16]{3,2,1,0:T(4,128)(2,1)S(1)} %bitcast.55) | data formatting | bytes 524288
  135.2 15.9 %all_to_all.29 = bf16[16,2,4096]{2,1,0:T(2,128)(2,1)S(1)} all-to-all(bf16[16,2,4096]{2,1,0:T(2,128)(2,1)S(1)} %reshape.157), channel_id=1, replica_groups=mesh['ep'=16,'tp'=16] {'tp'}, dimensions={0} | all-to-all | bytes 524288 | tf_op jit(solution)/shard_map/all_to_all | solution.py:72
  151.1 1.4 reshape.158
  152.6 1.6 copy.113
  154.2 1.1 copy.106
  155.3 6.5 %all-to-all-start.2 = ((bf16[16,128,64]{1,2,0:T(8,128)(2,1)}), bf16[16,128,64]{1,2,0:T(8,128)(2,1)S(1)}, u32[]{:S(2)}, u32[]{:S(2)}) async-start(bf16[16,128,64]{1,2,0:T(8,128)(2,1)} %copy.106), calls=%async_computation.2 | async-start | bytes 524288 | tf_op jit(solution)/shard_map/all_to_all | solution.py:74
  162.4 8.2 %all-to-all-done.2 = bf16[16,128,64]{1,2,0:T(8,128)(2,1)S(1)} async-done(((bf16[16,128,64]{1,2,0:T(8,128)(2,1)}), bf16[16,128,64]{1,2,0:T(8,128)(2,1)S(1)}, u32[]{:S(2)}, u32[]{:S(2)}) %all-to-all-start.2) | async-done | bytes 262176 | tf_op jit(solution)/shard_map/all_to_all | solution.py:74
  170.9 3.2 %gather_fusion = bf16[1024,64]{1,0:T(8,128)(2,1)S(1)} fusion(bf16[2048,64]{1,0:T(8,128)(2,1)S(1)} %bitcast.53, s32[1024]{0:T(1024)S(1)} %broadcast_clamp_fusion), kind=kCustom, calls=%fused_computation | custom fusion | bytes 266240 | tf_op jit(solution)/shard_map/gather | solution.py:77
  174.1 2.8 %fusion.3 = bf16[512,64]{1,0:T(8,128)(2,1)S(1)} fusion(bf16[512,2,64]{2,1,0:T(2,128)(2,1)S(1)} %bitcast.63, f32[512,2]{1,0:T(8,128)S(1)} %copy.85), kind=kLoop, calls=%fused_computation.8 | loop fusion | flops 163840 | bytes 200704 | tf_op jit(solution)/shard_map/reduce_sum | solution.py:78
  176.9 0.7 copy.109
  (46 shorter events, 5.1 us)
Async XLA Ops:
  6.5 7.1 %copy-start.2 = (s32[512,2]{0,1:T(2,128)S(1)}, s32[512,2]{0,1:T(2,128)}, u32[]{:S(2)}) copy-start(s32[512,2]{0,1:T(2,128)} %param.9) | copy-start | bytes 12292
  6.5 45.4 %all-gather.4.cloned.1.call-start = ((), (), s32[]{:S(2)}) async-start(), calls=%async_computation.3 | async-start | bytes 1114112 | tf_op jit(solution)/shard_map/all_gather | solution.py:56
  9.1 83.8 %all-gather.6.cloned.1.call-start = ((), (), s32[]{:S(2)}) async-start(), calls=%async_computation.4 | async-start | bytes 3342336 | tf_op jit(solution)/shard_map/all_gather | solution.py:17
  107.2 6.8 %copy-start = (bf16[16,32768]{1,0:T(8,128)(2,1)S(1)}, bf16[16,32768]{1,0:T(8,128)(2,1)}, u32[]{:S(2)}) copy-start(bf16[16,32768]{1,0:T(8,128)(2,1)} %get-tuple-element.9) | copy-start | bytes 3145732
  122.9 6.8 %copy-start.1 = (bf16[16,32768]{1,0:T(8,128)(2,1)S(1)}, bf16[16,32768]{1,0:T(8,128)(2,1)}, u32[]{:S(2)}) copy-start(bf16[16,32768]{1,0:T(8,128)(2,1)} %get-tuple-element.8) | copy-start | bytes 3145732
  151.1 11.0 %copy-start.3 = (f32[512,2]{0,1:T(2,128)S(1)}, f32[512,2]{0,1:T(2,128)}, u32[]{:S(2)}) copy-start(f32[512,2]{0,1:T(2,128)} %param.10) | copy-start | bytes 12292
  155.3 15.2 %all-to-all-start.2 = ((bf16[16,128,64]{1,2,0:T(8,128)(2,1)}), bf16[16,128,64]{1,2,0:T(8,128)(2,1)S(1)}, u32[]{:S(2)}, u32[]{:S(2)}) async-start(bf16[16,128,64]{1,2,0:T(8,128)(2,1)} %copy.106), calls=%async_computation.2 | async-start | bytes 524288 | tf_op jit(solution)/shard_map/all_to_all | solution.py:74
Sparse Core Ops, SparseCore 0:
  9.2 42.6 all-gather.3
  53.8 39.1 all-gather.5
where the time goes:
time: 185 us; the launch traced here: 184 us
  local copies, waits for them, and re-layouts  70.2 us (38%)
  waiting for transfers between devices  47.1 us (25%)
  blocking collectives  30.4 us (16%)
  other arithmetic  15.3 us (8%)
  between operations  13.7 us (7%)
  starting transfers between devices  6.57 us (4%)
    all_gather x1, waiting for transfers between devices, body(): group = lax.all_gather(normed, 'tp', axis=0, tiled=True)  27.5 us
    reshape x2, local copies, waits for them, and re-layouts, gather_together(): parts = lines[:, at:at + a.size].reshape(-1, *a.shape)  18.6 us
    all_to_all x1, blocking collectives, body(): lax.all_to_all(produced, 'tp', split_axis=3, concat_axis=2, tiled=True)  15.9 us
    all_to_all x1, blocking collectives, body(): landed = lax.all_to_all(mine, 'ep', split_axis=0, concat_axis=0, tiled=True)  14.5 us
    transpose x3, local copies, waits for them, and re-layouts, in_order(): return jnp.moveaxis(parts, 0, dim).reshape(shape)  13.7 us
    all_gather x1, waiting for transfers between devices, gather_together(): lines, at, outs = (lax.all_gather(flat, axis), 0, [])  11.4 us
    another operation x2, other arithmetic  9.04 us
    scatter x1, local copies, waits for them, and re-layouts, fill_buffer(): return buffer.at[flat_target].set(jnp.repeat(group, 2, axis=0))  8.55 us
  transfers between devices with their start and end apart: 3, of which 3 were waited for; matrix products, arithmetic and copies ran while one was open for 17% of the time, Pallas kernels for 0%

commit v1 on v0

v1 whole, which is shorter than its diff:
```python
import jax
import jax.numpy as jnp
from jax import lax
from jax.experimental import pallas as pl
from jax.experimental.pallas import tpu as pltpu
from jax.sharding import Mesh, PartitionSpec as P

epsilon = 1e-06
LANES = 128
F32 = jnp.float32
BF16 = jnp.bfloat16


def token_columns(first, rows, routing_ref, share_ref):
    count = routing_ref.shape[1]
    lane = lax.broadcasted_iota(jnp.int32, (rows, count), 1)
    row = lax.broadcasted_iota(jnp.int32, (rows, count), 0)
    hit = lane == row + first
    ids = [
        jnp.sum(jnp.where(hit, routing_ref[k : k + 1, :], 0), axis=1, keepdims=True) for k in (0, 1)
    ]
    shares = [
        jnp.sum(jnp.where(hit, share_ref[k : k + 1, :], 0.0), axis=1, keepdims=True) for k in (0, 1)
    ]
    return ids, shares


def pack_kernel(tp_ref, tokens_ref, gain_ref, routing_ref, share_ref, out_ref):
    copies, rows, _ = out_ref.shape
    width = tokens_ref.shape[1]
    as_float = tokens_ref[...].astype(F32)
    mean = jnp.mean(as_float * as_float, axis=-1, keepdims=True)
    normed = (as_float * lax.rsqrt(mean + epsilon) * gain_ref[...]).astype(BF16)
    ids, shares = token_columns(tp_ref[0] * rows, rows, routing_ref, share_ref)
    columns = [ids[0].astype(F32), ids[1].astype(F32)]
    for share in shares:
        high = share.astype(BF16).astype(F32)
        middle = (share - high).astype(BF16).astype(F32)
        low = share - high - middle
        columns += [high, middle, low]
    lane = lax.broadcasted_iota(jnp.int32, (rows, LANES), 1)
    extra = jnp.zeros((rows, LANES), F32)
    for at, column in enumerate(columns):
        extra = jnp.where(lane == at, column, extra)
    extra = extra.astype(BF16)
    for copy in range(copies):
        out_ref[copy, :, :width] = normed
        out_ref[copy, :, width:] = extra


def expert_kernel(ep_ref, rows_ref, own_ref, other_ref, out_ref):
    groups, rows, packed = rows_ref.shape
    width = packed - LANES
    local = own_ref.shape[2]
    everything = rows_ref[...].reshape(groups * rows, packed)
    x = everything[:, :width]
    extra = everything[:, width:].astype(F32)

    def weight(kind, expert):
        halves = [r[:, kind, expert].reshape(-1, width) for r in (own_ref, other_ref)]
        return jnp.concatenate(halves, axis=0)

    outs = []
    for expert in range(local):
        nt = (((1,), (1,)), ((), ()))
        gate = lax.dot_general(x, weight(0, expert), nt, preferred_element_type=F32)
        up = lax.dot_general(x, weight(1, expert), nt, preferred_element_type=F32)
        hidden = (gate / (1.0 + jnp.exp(-gate)) * up).astype(BF16)
        outs.append(jnp.dot(hidden, weight(2, expert), preferred_element_type=F32).astype(BF16))
    first = ep_ref[0] * local
    id0 = extra[:, 0:1].astype(jnp.int32) - first
    id1 = extra[:, 1:2].astype(jnp.int32) - first
    share0 = (extra[:, 2:3] + extra[:, 3:4]) + extra[:, 4:5]
    share1 = (extra[:, 5:6] + extra[:, 6:7]) + extra[:, 7:8]
    here0 = (id0 == 0) | (id0 == 1)
    here1 = (id1 == 0) | (id1 == 1)
    both = here0 & here1
    zero, one = outs[0].astype(F32), outs[1].astype(F32)
    pick0 = jnp.where(id0 == 0, zero, one)
    pick1 = jnp.where(id1 == 0, zero, one)
    mixed = share0 * pick0 + share1 * pick1
    result = jnp.where(both, mixed, jnp.where(here0, pick0, pick1))
    out_ref[...] = result.astype(BF16).reshape(groups, rows, width)


def combine_kernel(tp_ref, back_ref, routing_ref, share_ref, out_ref):
    sources, rows, width = back_ref.shape
    parts, _, columns = out_ref.shape
    ids, shares = token_columns(tp_ref[0] * rows, rows, routing_ref, share_ref)
    owner0, owner1 = ids[0] // 2, ids[1] // 2
    pick0 = jnp.zeros((rows, width), F32)
    pick1 = jnp.zeros((rows, width), F32)
    for source in range(sources):
        block = back_ref[source].astype(F32)
        pick0 = jnp.where(owner0 == source, block, pick0)
        pick1 = jnp.where(owner1 == source, block, pick1)
    mixed = shares[0] * pick0 + shares[1] * pick1
    result = jnp.where(owner0 == owner1, pick0, mixed).astype(BF16)
    for part in range(parts):
        out_ref[part] = result[:, part * columns : (part + 1) * columns]


def whole(*shape):
    return pl.BlockSpec(memory_space=pltpu.VMEM)


def body(tokens, norm_gain, routing, gate_share, w_gate, w_up, w_down):
    ep = ("y", "x")
    tp = ("z", "c")
    ep_size, tp_size = lax.axis_size(ep), lax.axis_size(tp)
    rows, width = tokens.shape
    ep_index = lax.axis_index(ep).astype(jnp.int32).reshape(1)
    tp_index = lax.axis_index(tp).astype(jnp.int32).reshape(1)
    routing_t, share_t = routing.T, gate_share.T
    smem = pl.BlockSpec(memory_space=pltpu.SMEM)
    vmem = pl.BlockSpec(memory_space=pltpu.VMEM)

    shards = jnp.stack([w_gate.transpose(0, 2, 1), w_up.transpose(0, 2, 1), w_down])
    own = lax.all_gather(shards, "z")

    packed = pl.pallas_call(
        pack_kernel,
        out_shape=jax.ShapeDtypeStruct((ep_size, rows, width + LANES), BF16),
        in_specs=[smem, vmem, vmem, vmem, vmem],
        out_specs=vmem,
        name="pack",
    )(tp_index, tokens, norm_gain.reshape(1, width), routing_t, share_t)
    landed = lax.all_to_all(packed, ep, 0, 0, tiled=True)
    own, landed = lax.optimization_barrier((own, landed))
    other = lax.ppermute(own, "c", [(0, 1), (1, 0)])
    produced = pl.pallas_call(
        expert_kernel,
        out_shape=jax.ShapeDtypeStruct((ep_size, rows, width), BF16),
        in_specs=[smem, vmem, vmem, vmem],
        out_specs=vmem,
        name="experts",
    )(ep_index, landed, own, other)
    back = lax.all_to_all(produced, ep, 0, 0, tiled=True)
    leaving = pl.pallas_call(
        combine_kernel,
        out_shape=jax.ShapeDtypeStruct((tp_size, rows, width // tp_size), BF16),
        in_specs=[smem, vmem, vmem, vmem],
        out_specs=vmem,
        name="combine",
    )(tp_index, back, routing_t, share_t)
    arrived = lax.all_to_all(leaving, tp, 0, 0, tiled=True)
    return arrived.reshape(tp_size * rows, width // tp_size)


def solution(mesh):
    ep, tp = ("y", "x"), ("z", "c")
    fine = Mesh(mesh.devices.reshape(4, 4, 8, 2), ep + tp)
    return jax.shard_map(
        body,
        mesh=fine,
        in_specs=(
            P(ep + tp, None),
            P(),
            P(ep, None),
            P(ep, None),
            P(ep, None, tp),
            P(ep, None, tp),
            P(ep, tp, None),
        ),
        out_specs=P(ep, tp),
        check_vma=False,
    )
```

time: 185 us -> 111 us (0.60)
  local copies, waits for them, and re-layouts: 70.2 us -> 3.06 us
  blocking collectives: 30.4 us -> 62.6 us
  waiting for transfers between devices: 47.1 us -> 15.3 us
  other arithmetic: 15.3 us -> 1.61 us
  Pallas kernels: 0 us -> 10.3 us
  starting transfers between devices: 6.57 us -> 4.72 us
    all_to_all x2 -> x3, blocking collectives: 30.4 us -> 62.6 us  [the longest x1 26 us: body(): landed = lax.all_to_all(packed, ep, 0, 0, tiled=True)]
    all_gather x2 -> x1, waiting for transfers between devices: 38.9 us -> 12.1 us  [body(): own = lax.all_gather(shards, 'z')]
    reshape x13 -> x1, local copies, waits for them, and re-layouts: 24.9 us -> 0.73 us  [body(): return arrived.reshape(tp_size * rows, width // tp_size)]
    transpose x4 -> x0, local copies, waits for them, and re-layouts: 13.9 us -> none  [the longest x3 13.7 us: in_order(): return jnp.moveaxis(parts, 0, dim).reshape(shape)]
    pallas_call x0 -> x3, Pallas kernels: none -> 10.3 us  [the longest x1 5.73 us: body(): pl.pallas_call(expert_kernel, out_shape=jax.ShapeDtypeStruct((ep_size, ro...]
    scatter x1 -> x0, local copies, waits for them, and re-layouts: 8.55 us -> none  [fill_buffer(): return buffer.at[flat_target].set(jnp.repeat(group, 2, axis=0))]
    all_to_all x1 -> x0, waiting for transfers between devices: 8.19 us -> none  [body(): lax.all_to_all(leaving, 'ep', split_axis=0, concat_axis=0, tiled=True)]
    another operation x2 -> x1, other arithmetic: 9.04 us -> 1.61 us  [body(): jnp.stack([w_gate.transpose(0, 2, 1), w_up.transpose(0, 2, 1), w_down])]
  transfers between devices with their start and end apart: 3 -> 2, of which waited for: 3 -> 2; matrix products, arithmetic and copies ran while one was open for 17% -> 0% of each run, Pallas kernels for 0% -> 2%
where the time goes in v1:
time: 111 us
  blocking collectives  62.6 us (56%)
  waiting for transfers between devices  15.3 us (14%)
  between operations  13.4 us (12%)
  Pallas kernels  10.3 us (9%)
  starting transfers between devices  4.72 us (4%)
  local copies, waits for them, and re-layouts  3.06 us (3%)
  other arithmetic  1.61 us (1%)
    all_to_all x1, blocking collectives, body(): landed = lax.all_to_all(packed, ep, 0, 0, tiled=True)  26 us
    all_to_all x1, blocking collectives, body(): back = lax.all_to_all(produced, ep, 0, 0, tiled=True)  23.3 us
    all_to_all x1, blocking collectives, body(): arrived = lax.all_to_all(leaving, tp, 0, 0, tiled=True)  13.3 us
    all_gather x1, waiting for transfers between devices, body(): own = lax.all_gather(shards, 'z')  12.1 us
    pallas_call x1, Pallas kernels, body(): pl.pallas_call(expert_kernel, out_shape=jax.ShapeDtypeStruct((ep_size, ro...  5.73 us
    ppermute x1, starting transfers between devices, body(): other = lax.ppermute(own, 'c', [(0, 1), (1, 0)])  4.72 us
    ppermute x1, waiting for transfers between devices, body(): other = lax.ppermute(own, 'c', [(0, 1), (1, 0)])  3.25 us
    pallas_call x1, Pallas kernels, body(): pl.pallas_call(combine_kernel, out_shape=jax.ShapeDtypeStruct((tp_size, r...  2.45 us
  transfers between devices with their start and end apart: 2, of which 2 were waited for; matrix products, arithmetic and copies ran while one was open for 0% of the time, Pallas kernels for 2%

profile of v1, /device:TPU:1, one launch (start us, length us, event | category | flops | bytes accessed | tf_op | source)
XLA Modules:
  0.0 111.0 jit_solution(9421068311074293557)
XLA Ops:
  6.5 0.0 all-gather.3.cloned.1.call-start
  6.5 1.6 %pad_maximum_fusion = bf16[3,2,16,1024]{3,2,1,0:T(8,128)(2,1)} fusion(bf16[1,2,16,1024]{3,2,1,0:T(8,128)(2,1)} %bitcast.17, bf16[1,2,16,1024]{3,2,1,0:T(8,128)(2,1)} %bitcast.18, bf16[1,2,16,1024]{3,2,1,0:T(8,128)(2,1)} %bitcast.19), kind=kLoop, calls=%fused_computation | loop fusion | flops 196608 | bytes 393216 | tf_op jit(solution)/shard_map/stack | solution.py:118
  8.1 0.0 all-gather.3.cloned.1.call-update
  8.2 2.1 %pack.1 = bf16[16,32,1152]{2,1,0:T(8,128)(2,1)} custom-call(s32[1]{0:T(128)} %bitcast.tp_ref, bf16[32,1024]{1,0:T(8,128)(2,1)} %tokens_ref.1, f32[1,1024]{1,0:T(1,128)} %bitcast.24, s32[2,512]{1,0:T(2,128)} %bitcast.20, f32[2,512]{1,0:T(2,128)} %bitcast.22), custom_call_target="tpu_custom_call" | custom-call | tf_op jit(solution)/shard_map/pack/pallas_call | solution.py:121
  10.3 26.0 %all_to_all.15.rows_ref = bf16[16,32,1152]{2,1,0:T(8,128)(2,1)} all-to-all(bf16[16,32,1152]{2,1,0:T(8,128)(2,1)} %pack.1), channel_id=1, replica_groups=mesh['y'=4,'x'=4,'z'=8,'c'=2] {'y','x'}, dimensions={0} | all-to-all | bytes 2359296 | tf_op jit(solution)/shard_map/all_to_all | solution.py:128
  36.3 12.1 %all-gather.3.cloned.1.call-done = bf16[24,2,16,1024]{3,2,1,0:T(8,128)(2,1)} async-done(((bf16[3,2,16,1024]{3,2,1,0:T(8,128)(2,1)}), bf16[24,2,16,1024]{3,2,1,0:T(8,128)(2,1)}) %all-gather.3.cloned.1.call-update) | async-done | bytes 1572880 | tf_op jit(solution)/shard_map/all_gather | solution.py:119
  48.3 4.7 %collective-permute-start = (bf16[8,3,2,16,1024]{4,3,2,1,0:T(8,128)(2,1)}, bf16[8,3,2,16,1024]{4,3,2,1,0:T(8,128)(2,1)S(1)}, u32[]{:S(2)}, u32[]{:S(2)}) collective-permute-start(bf16[8,3,2,16,1024]{4,3,2,1,0:T(8,128)(2,1)} %bitcast.14), channel_id=1, source_target_pairs={{0,1},{1,0},{2,3},{3,2},{4,5},{5,4},{6,7},{7,6},{8,9},{9,8},{10,11... | collective-permute-start | bytes 4718600 | tf_op jit(solution)/shard_map/ppermute | solution.py:130
  53.0 3.2 %collective-permute-done.other_ref = bf16[8,3,2,16,1024]{4,3,2,1,0:T(8,128)(2,1)S(1)} collective-permute-done((bf16[8,3,2,16,1024]{4,3,2,1,0:T(8,128)(2,1)}, bf16[8,3,2,16,1024]{4,3,2,1,0:T(8,128)(2,1)S(1)}, u32[]{:S(2)}, u32[]{:S(2)}) %collective-permute-start) | collective-permute-done | bytes 1572896 | tf_op jit(solution)/shard_map/ppermute | solution.py:130
  56.3 0.0 copy-start
  56.3 1.1 %copy-done = bf16[8,3,2,16,1024]{4,3,2,1,0:T(8,128)(2,1)} copy-done((bf16[8,3,2,16,1024]{4,3,2,1,0:T(8,128)(2,1)}, bf16[8,3,2,16,1024]{4,3,2,1,0:T(8,128)(2,1)S(1)}, u32[]{:S(2)}) %copy-start) | copy-done | bytes 1572888
  57.4 5.7 %experts.1 = bf16[16,32,1024]{2,1,0:T(8,128)(2,1)} custom-call(s32[1]{0:T(128)} %bitcast.1.ep_ref, bf16[16,32,1152]{2,1,0:T(8,128)(2,1)} %all_to_all.15.rows_ref, bf16[8,3,2,16,1024]{4,3,2,1,0:T(8,128)(2,1)} %bitcast.15, bf16[8,3,2,16,1024]{4,3,2,1,0:T(8,128)(2,1)} %copy-done), custom_call_target="tpu_custom_call" | custom-call | tf_op jit(solution)/shard_map/experts/pallas_call | solution.py:131
  63.2 23.3 %all_to_all.16.back_ref = bf16[16,32,1024]{2,1,0:T(8,128)(2,1)} all-to-all(bf16[16,32,1024]{2,1,0:T(8,128)(2,1)} %experts.1), channel_id=1, replica_groups=mesh['y'=4,'x'=4,'z'=8,'c'=2] {'y','x'}, dimensions={0} | all-to-all | bytes 2097152 | tf_op jit(solution)/shard_map/all_to_all | solution.py:138
  86.5 2.4 %combine.1 = bf16[16,32,64]{2,1,0:T(8,128)(2,1)} custom-call(s32[1]{0:T(128)} %bitcast.tp_ref, bf16[16,32,1024]{2,1,0:T(8,128)(2,1)} %all_to_all.16.back_ref, s32[2,512]{1,0:T(2,128)} %bitcast.21, f32[2,512]{1,0:T(2,128)} %bitcast.23), custom_call_target="tpu_custom_call" | custom-call | tf_op jit(solution)/shard_map/combine/pallas_call | solution.py:139
  88.9 1.0 reshape.17
  90.0 13.3 %all_to_all.17 = bf16[16,2,1024]{2,1,0:T(2,128)(2,1)S(1)} all-to-all(bf16[16,2,1024]{2,1,0:T(2,128)(2,1)S(1)} %reshape.17), channel_id=1, replica_groups=mesh['y'=4,'x'=4,'z'=8,'c'=2] {'z','c'}, dimensions={0} | all-to-all | bytes 131072 | tf_op jit(solution)/shard_map/all_to_all | solution.py:146
  103.2 0.1 reshape.18
  103.4 0.7 copy.9
Async XLA Ops:
  6.5 41.8 %all-gather.3.cloned.1.call-start = ((), (), s32[]{:S(2)}) async-start(), calls=%async_computation.3 | async-start | bytes 1769472 | tf_op jit(solution)/shard_map/all_gather | solution.py:119
  48.3 8.0 %collective-permute-start = (bf16[8,3,2,16,1024]{4,3,2,1,0:T(8,128)(2,1)}, bf16[8,3,2,16,1024]{4,3,2,1,0:T(8,128)(2,1)S(1)}, u32[]{:S(2)}, u32[]{:S(2)}) collective-permute-start(bf16[8,3,2,16,1024]{4,3,2,1,0:T(8,128)(2,1)} %bitcast.14), channel_id=1, source_target_pairs={{0,1},{1,0},{2,3},{3,2},{4,5},{5,4},{6,7},{7,6},{8,9},{9,8},{10,11... | collective-permute-start | bytes 4718600 | tf_op jit(solution)/shard_map/ppermute | solution.py:130
  56.3 1.2 %copy-start = (bf16[8,3,2,16,1024]{4,3,2,1,0:T(8,128)(2,1)}, bf16[8,3,2,16,1024]{4,3,2,1,0:T(8,128)(2,1)S(1)}, u32[]{:S(2)}) copy-start(bf16[8,3,2,16,1024]{4,3,2,1,0:T(8,128)(2,1)S(1)} %collective-permute-done.other_ref) | copy-start | bytes 4718596
Sparse Core Ops, SparseCore 0:
  9.1 39.1 all-gather.2
